TPU v7x, 32 devices: a whole 2x2x4 slice. The times are simulated.
32 devices in a mesh: grp: 2 (over y), tp: 4 (over z), dp: 4 (over x, core).
Axes of the slice: x: 2, y: 2, z: 4, core: 2. Of those that a mesh axis runs over, the one named last changes fastest.
Arguments:
- tokens: bfloat16 [512, 4096], P('grp', 'dp'), parts along dimension 0, may hold values from -40 to 40
- sequence_lengths: int32 [512], P(('grp', 'dp')), parts along dimension 0, may hold values from 1 to 4096, 262144 in all
- recurrent_state: float32 [2, 512, 128, 128], P(None, ('grp', 'dp'), 'tp'), parts along dimension 1, may hold values from -1.8 to 1.8
- norm_weight: float32 [2, 4096], P(None, 'dp'), may hold values from 0.1 to 1.9
- input_weight: bfloat16 [2, 4096, 2048], P(None, 'dp', 'tp'), may hold values from -0.09375 to 0.09375
- gate_weight: bfloat16 [2, 4096, 2048], P(None, 'dp', 'tp'), may hold values from -0.09375 to 0.09375
- output_weight: bfloat16 [2, 2048, 4096], P(None, 'tp', 'dp'), may hold values from -0.125 to 0.125
- negated_real_rate: float32 [2, 8192], P(None, 'tp'), may hold values from 0.005 to 1
- frequency: float32 [2, 8192], P(None, 'tp'), may hold values from -4 to 4
- discrete_step: float32 [2, 128], P(None, 'tp'), may hold values from 0.02 to 0.5
- group_input_matrix: float32 [2, 128, 16, 128], P(None, 'tp'), may hold values from -1.5 to 1.5
- group_output_matrix: float32 [2, 128, 16, 128], P(None, 'tp'), may hold values from -0.5 to 0.5
- feedthrough_weight: float32 [2, 2048], P(None, 'tp'), may hold values from -3 to 3
- extra_log_decay: float32 [2, 128, 4096], P(None, 'tp'), may hold values from -0.7 to 0
Outputs:
- tokens_out: bfloat16 [512, 4096], P('grp', 'dp'), parts along dimension 0
- state_out: float32 [2, 512, 128, 128], P(None, ('grp', 'dp'), 'tp'), parts along dimension 1
There are 2 independent parts, one for each index of `grp`. A program takes and returns all parts, laid end to end along the dimension named above; an argument that names none is the same for every part. Nothing has to cross between parts.
Inputs may be any that keep to these rules, and one draw needn't show every extreme that they name: The newest token of a sequence stands at position sequence_lengths - 1.
All inputs are finite; a program needn't handle non-finite values. No bound on the sum of `sequence_lengths` on one device may be relied on, other than what follows from the above.
Results may differ from a plain program's by a relative error of at most 0.009.
Values may be sent and summed in bfloat16 or wider, within the bound.
A program may use at most 64 MiB of HBM per device.

v0:
```python
import jax
import jax.numpy as jnp
from jax import lax
from jax.sharding import PartitionSpec as P

D = 4096
STACKED_LAYERS = 2
TOP_PRECISION = lax.Precision.HIGHEST
NORM_EPS = 1e-06


def transition(decay_factor, angular_frequency, step_width):
    log_mag = -decay_factor * step_width[:, None]
    turn = angular_frequency * step_width[:, None]
    magnitude = jnp.exp(log_mag)
    discrete_real = magnitude * jnp.cos(turn)
    discrete_imaginary = magnitude * jnp.sin(turn)
    half_sine = jnp.sin(0.5 * turn)
    numer_re = jnp.expm1(log_mag) * jnp.cos(turn) - 2.0 * half_sine * half_sine
    denom = decay_factor * decay_factor + angular_frequency * angular_frequency
    drive_re = (-numer_re * decay_factor + discrete_imaginary * angular_frequency) / denom
    drive_im = (-discrete_imaginary * decay_factor - numer_re * angular_frequency) / denom
    return (discrete_real, discrete_imaginary, drive_re, drive_im)


def state_space_update(
    input_groups,
    layer_state,
    extra_decay_factor,
    decay_factor,
    angular_frequency,
    step_width,
    input_matrix,
    readout_matrix,
):
    half_width = input_matrix.shape[-1] // 2
    decay_factor = decay_factor.reshape(-1, half_width)
    angular_frequency = angular_frequency.reshape(-1, half_width)
    discrete_real, discrete_imaginary, drive_re, drive_im = transition(
        decay_factor, angular_frequency, step_width
    )
    input_real = input_matrix[..., :half_width]
    input_imaginary = input_matrix[..., half_width:]
    driven_input_real = jnp.einsum(
        "tkl,klf->tkf", input_groups, input_real, precision=TOP_PRECISION
    )
    driven_input_imaginary = jnp.einsum(
        "tkl,klf->tkf", input_groups, input_imaginary, precision=TOP_PRECISION
    )
    state_re = layer_state[..., :half_width]
    state_im = layer_state[..., half_width:]
    carried_real = extra_decay_factor[..., None] * discrete_real[None]
    carried_imaginary = extra_decay_factor[..., None] * discrete_imaginary[None]
    updated_real = (
        carried_real * state_re
        - carried_imaginary * state_im
        + drive_re[None] * driven_input_real
        - drive_im[None] * driven_input_imaginary
    )
    updated_imaginary = (
        carried_real * state_im
        + carried_imaginary * state_re
        + drive_re[None] * driven_input_imaginary
        + drive_im[None] * driven_input_real
    )
    readout_rows = jnp.einsum(
        "hzk,dhk->dhz", readout_matrix[..., :half_width], updated_real, precision=TOP_PRECISION
    ) - jnp.einsum(
        "hzk,dhk->dhz", readout_matrix[..., half_width:], updated_imaginary, precision=TOP_PRECISION
    )
    return (readout_rows, jnp.concatenate([updated_real, updated_imaginary], axis=-1))


def single_layer(
    hidden_rows,
    sequence_lengths,
    layer_state,
    norm_scale_rows,
    input_matrix_weight,
    gate_matrix,
    output_matrix_weight,
    decay_factor,
    angular_frequency,
    step_width,
    input_matrix,
    readout_matrix,
    feedthrough_rows,
    extra_decay_rows,
):
    x_float = hidden_rows.astype(jnp.float32)
    square_sums = jnp.sum(x_float * x_float, axis=1)
    scaled_in = (x_float * norm_scale_rows[None, :]).astype(jnp.bfloat16)
    input_part = jnp.dot(scaled_in, input_matrix_weight, preferred_element_type=jnp.float32)
    gate_part = jnp.dot(scaled_in, gate_matrix, preferred_element_type=jnp.float32)
    local_rows = sequence_lengths.shape[0]
    input_sum, gate_sum, mine_squares = (
        lax.psum_scatter(input_part, "dp", scatter_dimension=0, tiled=True),
        lax.psum_scatter(gate_part, "dp", scatter_dimension=0, tiled=True),
        lax.psum_scatter(square_sums, "dp", scatter_dimension=0, tiled=True),
    )
    scale = lax.rsqrt(mine_squares / D + NORM_EPS)[:, None]
    u_vals = (input_sum * scale).astype(jnp.bfloat16)
    gate_vals = (gate_sum * scale).astype(jnp.bfloat16)
    group_count = layer_state.shape[1]
    input_float = u_vals.astype(jnp.float32)
    token_positions = sequence_lengths - 1
    extra_decay_factor = jnp.exp(jnp.take(extra_decay_rows, token_positions, axis=1).T)
    readout_rows, updated_state = state_space_update(
        input_float.reshape(local_rows, group_count, -1),
        layer_state,
        extra_decay_factor,
        decay_factor,
        angular_frequency,
        step_width,
        input_matrix,
        readout_matrix,
    )
    y_vals = jax.nn.gelu(
        readout_rows.reshape(local_rows, -1) + feedthrough_rows[None, :] * input_float
    )
    mixed = (y_vals * jax.nn.sigmoid(gate_vals.astype(jnp.float32))).astype(jnp.bfloat16)
    branch_terms = jnp.dot(
        lax.all_gather(mixed, "dp", axis=0, tiled=True),
        output_matrix_weight,
        preferred_element_type=jnp.float32,
    )
    branch = lax.psum(branch_terms, "tp").astype(jnp.bfloat16)
    x_next = (x_float + branch.astype(jnp.float32)).astype(jnp.bfloat16)
    return (x_next, updated_state)


def on_device(
    tokens,
    sequence_lengths,
    recurrent_state,
    norm_weight,
    input_weight,
    gate_weight,
    output_weight,
    negated_real_rate,
    frequency,
    discrete_step,
    group_input_matrix,
    group_output_matrix,
    feedthrough_weight,
    extra_log_decay,
):
    hidden_rows = tokens
    states = []
    for index_of_layer in range(STACKED_LAYERS):
        hidden_rows, updated_state = single_layer(
            hidden_rows,
            sequence_lengths,
            recurrent_state[index_of_layer],
            norm_weight[index_of_layer],
            input_weight[index_of_layer],
            gate_weight[index_of_layer],
            output_weight[index_of_layer],
            negated_real_rate[index_of_layer],
            frequency[index_of_layer],
            discrete_step[index_of_layer],
            group_input_matrix[index_of_layer],
            group_output_matrix[index_of_layer],
            feedthrough_weight[index_of_layer],
            extra_log_decay[index_of_layer],
        )
        states.append(updated_state)
    return (hidden_rows, jnp.stack(states, axis=0))


def solution(mesh):
    in_specs = (
        P("grp", "dp"),
        P(("grp", "dp")),
        P(None, ("grp", "dp"), "tp", None),
        P(None, "dp"),
        P(None, "dp", "tp"),
        P(None, "dp", "tp"),
        P(None, "tp", "dp"),
        P(None, "tp"),
        P(None, "tp"),
        P(None, "tp"),
        P(None, "tp", None, None),
        P(None, "tp", None, None),
        P(None, "tp"),
        P(None, "tp", None),
    )
    out_specs = (P("grp", "dp"), P(None, ("grp", "dp"), "tp", None))
    return jax.shard_map(
        on_device, mesh=mesh, in_specs=in_specs, out_specs=out_specs, check_vma=False
    )
```

profile of v0, /device:TPU:0, one launch (start us, length us, event | category | flops | bytes accessed | tf_op | source)
XLA Modules:
  0.0 220.6 jit_solution(5358436251447161086)
XLA Ops:
  7.2 0.8 fusion.85
  8.0 2.6 %fusion.28 = f32[256,512]{1,0:T(8,128)} fusion(bf16[2,1024,512]{2,1,0:T(8,128)(2,1)} %param.20, bf16[256,1024]{1,0:T(8,128)(2,1)} %param.16, f32[1024]{0:T(1024)S(1)} %bitcast.103), kind=kOutput, calls=%fused_computation.51 | convolution fusion | flops 269221888 | bytes 2101248 | tf_op jit(solution)/shard_map/dot_general | solution.py:93
  10.7 0.0 reduce-scatter.7.cloned.1.call-start
  10.8 2.6 %fusion.26 = f32[256,512]{1,0:T(8,128)} fusion(bf16[2,1024,512]{2,1,0:T(8,128)(2,1)} %param.21, bf16[256,1024]{1,0:T(8,128)(2,1)S(1)} %copy-done.3, f32[1024]{0:T(1024)S(1)} %bitcast.104), kind=kOutput, calls=%fused_computation.49 | convolution fusion | flops 269221888 | bytes 2101248 | tf_op jit(solution)/shard_map/dot_general | solution.py:94
  13.4 0.2 fusion.13
  13.6 8.5 %all-reduce = f32[256]{0:T(256)S(1)} all-reduce(f32[256]{0:T(256)S(1)} %fusion.13), channel_id=3, replica_groups=mesh['grp'=2,'tp'=4,'dp'=4] {'dp'}, use_global_device_ids=true, to_apply=%region_2.4.clone | all-reduce | flops 256 | bytes 2048
  22.2 0.1 slice_reduce_fusion
  22.3 0.1 reshape_squeeze.13
  22.4 0.1 reshape_squeeze.12
  22.5 0.7 slice_bitcast_fusion.1
  23.2 0.9 fusion.84
  24.1 1.6 copy.53
  25.8 1.9 copy.51
  27.7 0.6 gather_fusion.1
  28.3 2.3 %gather_fusion = f32[64,32]{1,0:T(8,128)S(1)} fusion(f32[32,4096]{0,1:T(8,128)} %bitcast.92, s32[1024]{0:T(1024)S(1)} %pad_clamp_fusion), kind=kCustom, calls=%fused_computation.clone | custom fusion | bytes 16640 | tf_op jit(solution)/shard_map/jit(_take)/gather | solution.py:107
  30.5 0.1 fusion.72
  30.6 0.1 copy.41
  30.7 1.7 fusion.83
  32.5 0.6 dynamic-slice
  33.7 0.1 fusion.80
  33.8 2.5 %copy_bitcast_fusion = (f32[64,32,128]{2,0,1:T(8,128)}, f32[64,32,128]{2,0,1:T(8,128)}) fusion(f32[1,64,32,128]{3,2,1,0:T(8,128)S(1)} %get-tuple-element.21, f32[1,64,32,128]{3,2,1,0:T(8,128)S(1)} %get-tuple-element.22), kind=kLoop, calls=%fused_computation.39 | loop fusion | bytes 4194304 | tf_op jit(solution)/shard_map/squeeze | solution.py:154
  36.3 0.2 exponential_multiply_fusion.1
  36.5 1.0 multiply_convert_fusion.3
  37.5 0.1 copy.43
  37.7 0.8 fusion.50
  38.5 2.8 %fusion.5 = (f32[64,32,64]{2,0,1:T(8,128)S(1)}, f32[64,32,64]{2,0,1:T(8,128)S(1)}) fusion(f32[32,64,64]{2,1,0:T(8,128)S(1)} %fusion.50, f32[64,32,128]{2,0,1:T(8,128)} %get-tuple-element.46, f32[32,64]{1,0:T(8,128)S(1)} %get-tuple-element.36, f32[32,64]{1,0:T(8,128)S(1)} %get-tuple-element.35, f32[32,64]{1,0:T(8,128)S(1)} %get-tuple-element.34, ...), kind=kOutput, calls=%fused_computation.24 | convolution fusion | flops 27262976 | bytes 2990080 | tf_op jit(solution)/shard_map/tkl,klf->tkf/dot_general | solution.py:44
  41.3 1.7 fusion.48
  43.0 1.8 convolution_subtract_fusion.1
  44.8 0.1 copy.44
  45.0 14.7 %reduce-scatter.7.cloned.1.call-done = f32[64,512]{1,0:T(8,128)} async-done(((f32[256,512]{1,0:T(8,128)}), f32[64,512]{1,0:T(8,128)}) %reduce-scatter.7.cloned.1.call-update) | async-done | bytes 131088 | tf_op jit(solution)/shard_map/reduce_scatter | solution.py:98
  59.6 1.1 fusion.62
  60.7 5.8 %all_gather.6 = bf16[256,512]{1,0:T(8,128)(2,1)S(1)} all-gather(bf16[64,512]{1,0:T(8,128)(2,1)S(1)} %fusion.62), channel_id=1, replica_groups=mesh['grp'=2,'tp'=4,'dp'=4] {'dp'}, dimensions={0}, use_global_device_ids=true | all-gather | bytes 327680 | tf_op jit(solution)/shard_map/all_gather | solution.py:123
  66.5 1.7 fusion.24
  68.1 44.3 %all-reduce.4 = bf16[256,1024]{1,0:T(8,128)(2,1)} all-reduce(f32[256,1024]{1,0:T(8,128)S(1)} %fusion.24), channel_id=1, replica_groups=mesh['grp'=2,'tp'=4,'dp'=4] {'tp'}, use_global_device_ids=true, to_apply=%region_4.0 | all-reduce | flops 262144 | bytes 1572864 | tf_op jit(solution)/shard_map/psum | solution.py:127
  112.4 1.5 fusion.16
  113.9 2.7 %fusion.22 = f32[256,512]{1,0:T(8,128)} fusion(bf16[2,1024,512]{2,1,0:T(8,128)(2,1)} %param.20, bf16[256,1024]{1,0:T(8,128)(2,1)S(1)} %get-tuple-element.14, f32[1024]{0:T(1024)S(1)} %bitcast.101), kind=kOutput, calls=%fused_computation.45 | convolution fusion | flops 269221888 | bytes 2101248 | tf_op jit(solution)/shard_map/dot_general | solution.py:93
  116.6 0.0 reduce-scatter.11.cloned.1.call-start
  116.6 0.1 reshape_squeeze.15
  116.7 0.1 reshape_squeeze.14
  116.8 0.1 copy.46
  116.8 0.2 exponential_multiply_fusion
  117.1 6.2 %all-reduce.1 = f32[256]{0:T(256)S(1)} all-reduce(f32[256]{0:T(256)S(1)} %get-tuple-element.13), channel_id=6, replica_groups=mesh['grp'=2,'tp'=4,'dp'=4] {'dp'}, use_global_device_ids=true, to_apply=%region_7.9.clone | all-reduce | flops 256 | bytes 2048
  123.2 0.1 fusion.81
  123.3 0.3 maximum_bitcast_fusion
  123.6 1.2 copy-done.15
  124.8 0.1 copy-done.2
  124.9 1.2 fusion.20
  126.2 10.6 %reduce-scatter.9.cloned.1.call-done = f32[64,512]{1,0:T(8,128)} async-done(((f32[256,512]{1,0:T(8,128)}), f32[64,512]{1,0:T(8,128)}) %reduce-scatter.9.cloned.1.call-update) | async-done | bytes 131088 | tf_op jit(solution)/shard_map/reduce_scatter | solution.py:97
  136.8 1.0 multiply_convert_fusion.1
  137.8 0.1 copy.48
  137.9 0.8 fusion.43
  138.7 1.5 fusion.11
  140.2 0.3 maximum_bitcast_fusion.1
  140.5 0.2 pad_maximum_fusion
  140.8 2.5 %copy.50 = f32[2,64,32,128]{3,2,1,0:T(8,128)} copy(f32[2,64,32,128]{3,1,2,0:T(8,128)S(1)} %pad_maximum_fusion) | data formatting | bytes 4194304
  143.3 1.7 fusion.41
  145.0 1.8 convolution_subtract_fusion
  146.9 0.1 copy.49
  147.0 13.8 %reduce-scatter.11.cloned.1.call-done = f32[64,512]{1,0:T(8,128)} async-done(((f32[256,512]{1,0:T(8,128)}), f32[64,512]{1,0:T(8,128)}) %reduce-scatter.11.cloned.1.call-update) | async-done | bytes 131088 | tf_op jit(solution)/shard_map/reduce_scatter | solution.py:98
  160.8 1.1 fusion.71
  161.9 5.8 %all_gather.7 = bf16[256,512]{1,0:T(8,128)(2,1)S(1)} all-gather(bf16[64,512]{1,0:T(8,128)(2,1)S(1)} %fusion.71), channel_id=1, replica_groups=mesh['grp'=2,'tp'=4,'dp'=4] {'dp'}, dimensions={0}, use_global_device_ids=true | all-gather | bytes 327680 | tf_op jit(solution)/shard_map/all_gather | solution.py:123
  167.7 0.4 fusion.18
  168.1 43.9 %all-reduce.5 = bf16[256,1024]{1,0:T(8,128)(2,1)S(1)} all-reduce(f32[256,1024]{1,0:T(8,128)S(1)} %fusion.18), channel_id=1, replica_groups=mesh['grp'=2,'tp'=4,'dp'=4] {'tp'}, use_global_device_ids=true, to_apply=%region_9.11 | all-reduce | flops 262144 | bytes 1572864 | tf_op jit(solution)/shard_map/psum | solution.py:127
  212.0 2.0 fusion.17
  (46 shorter events, 0.3 us)
Async XLA Ops:
  7.2 3.6 %copy-start.3 = (bf16[256,1024]{1,0:T(8,128)(2,1)S(1)}, bf16[256,1024]{1,0:T(8,128)(2,1)}, u32[]{:S(2)}) copy-start(bf16[256,1024]{1,0:T(8,128)(2,1)} %param.16) | copy-start | bytes 1572868
  7.2 29.4 %reduce-scatter.5.cloned.1.call-start = ((), (), s32[]{:S(2)}) async-start(), calls=%async_computation.4 | async-start | bytes 655360 | tf_op jit(solution)/shard_map/reduce_scatter | solution.py:97
  10.6 11.5 %copy-start.16 = (s32[64]{0:T(128)S(1)}, s32[64]{0:T(128)}, u32[]{:S(2)}) copy-start(s32[64]{0:T(128)} %param.17) | copy-start | bytes 772
  10.6 11.5 %copy-start.14 = (f32[2,32]{1,0:T(2,128)S(1)}, f32[2,32]{1,0:T(2,128)}, u32[]{:S(2)}) copy-start(f32[2,32]{1,0:T(2,128)} %param.25) | copy-start | bytes 772
  10.6 11.5 %copy-start.13 = (f32[2,512]{1,0:T(2,128)S(1)}, f32[2,512]{1,0:T(2,128)}, u32[]{:S(2)}) copy-start(f32[2,512]{1,0:T(2,128)} %param.28) | copy-start | bytes 12292
  10.6 11.6 %copy-start.11 = (f32[2,2048]{1,0:T(2,128)S(1)}, f32[2,2048]{1,0:T(2,128)}, u32[]{:S(2)}) copy-start(f32[2,2048]{1,0:T(2,128)} %param.24) | copy-start | bytes 49156
  10.7 11.6 %copy-start.12 = (f32[2,2048]{1,0:T(2,128)S(1)}, f32[2,2048]{1,0:T(2,128)}, u32[]{:S(2)}) copy-start(f32[2,2048]{1,0:T(2,128)} %param.23) | copy-start | bytes 49156
  10.7 11.8 %copy-start.7 = (f32[2,32,16,128]{3,2,1,0:T(8,128)S(1)}, f32[2,32,16,128]{3,2,1,0:T(8,128)}, u32[]{:S(2)}) copy-start(f32[2,32,16,128]{3,2,1,0:T(8,128)} %param.26) | copy-start | bytes 1572868
  10.7 12.5 %copy-start.8 = (f32[2,32,16,128]{3,2,1,0:T(8,128)S(1)}, f32[2,32,16,128]{3,2,1,0:T(8,128)}, u32[]{:S(2)}) copy-start(f32[2,32,16,128]{3,2,1,0:T(8,128)} %param.27) | copy-start | bytes 1572868
  10.7 48.9 %reduce-scatter.7.cloned.1.call-start = ((), (), s32[]{:S(2)}) async-start(), calls=%async_computation.5 | async-start | bytes 655360 | tf_op jit(solution)/shard_map/reduce_scatter | solution.py:98
  13.4 9.9 %copy-start.4 = (f32[2,32,4096]{2,1,0:T(8,128)S(1)}, f32[2,32,4096]{2,1,0:T(8,128)}, u32[]{:S(2)}) copy-start(f32[2,32,4096]{2,1,0:T(8,128)} %param.29) | copy-start | bytes 3145732
  13.4 123.4 %reduce-scatter.9.cloned.1.call-start = ((), (), s32[]{:S(2)}) async-start(), calls=%async_computation.6 | async-start | bytes 655360 | tf_op jit(solution)/shard_map/reduce_scatter | solution.py:97
  30.7 1.8 copy-start.17
  41.3 18.3 %copy-start.9 = (f32[64,512]{1,0:T(8,128)S(1)}, f32[64,512]{1,0:T(8,128)}, u32[]{:S(2)}) copy-start(f32[64,512]{1,0:T(8,128)} %reduce-scatter.5.cloned.1.call-done) | copy-start | bytes 393220
  113.9 9.3 %copy-start.1 = (bf16[256,1024]{1,0:T(8,128)(2,1)}, bf16[256,1024]{1,0:T(8,128)(2,1)S(1)}, u32[]{:S(2)}) copy-start(bf16[256,1024]{1,0:T(8,128)(2,1)S(1)} %get-tuple-element.14) | copy-start | bytes 1572868
  116.6 44.2 %reduce-scatter.11.cloned.1.call-start = ((), (), s32[]{:S(2)}) async-start(), calls=%async_computation.7 | async-start | bytes 655360 | tf_op jit(solution)/shard_map/reduce_scatter | solution.py:98
  123.2 1.6 copy-start.15
  123.3 1.6 copy-start.2
  124.9 13.0 %copy-start.6 = (f32[32,16,128]{2,1,0:T(8,128)S(1)}, f32[32,16,128]{2,1,0:T(8,128)}, u32[]{:S(2)}) copy-start(f32[32,16,128]{2,1,0:T(8,128)} %get-tuple-element.27) | copy-start | bytes 786436
  124.9 13.8 %copy-start.5 = (f32[64,32,128]{2,0,1:T(8,128)S(1)}, f32[64,32,128]{2,0,1:T(8,128)}, u32[]{:S(2)}) copy-start(f32[64,32,128]{2,0,1:T(8,128)} %get-tuple-element.45) | copy-start | bytes 3145732
  143.3 17.5 %copy-start.10 = (f32[64,512]{1,0:T(8,128)S(1)}, f32[64,512]{1,0:T(8,128)}, u32[]{:S(2)}) copy-start(f32[64,512]{1,0:T(8,128)} %reduce-scatter.9.cloned.1.call-done) | copy-start | bytes 393220
  143.3 24.3 %copy-start = (bf16[2,512,1024]{2,1,0:T(8,128)(2,1)S(1)}, bf16[2,512,1024]{2,1,0:T(8,128)(2,1)}, u32[]{:S(2)}) copy-start(bf16[2,512,1024]{2,1,0:T(8,128)(2,1)} %param.22) | copy-start | bytes 6291460
Sparse Core Ops, SparseCore 0:
  11.0 24.3 reduce-scatter.4
  38.0 21.6 reduce-scatter.6
  116.7 20.0 reduce-scatter.8
  139.1 21.6 reduce-scatter.10
where the time goes:
time: 221 us
  blocking collectives  114 us (52%)
  waiting for transfers between devices  39.2 us (18%)
  matrix products  24.2 us (11%)
  local copies, waits for them, and re-layouts  18.5 us (8%)
  between operations  14.8 us (7%)
  other arithmetic  9.38 us (4%)
    psum x2, blocking collectives, single_layer(): branch = lax.psum(branch_terms, 'tp').astype(jnp.bfloat16)  88.2 us
    reduce_scatter x2, waiting for transfers between devices, single_layer(): lax.psum_scatter(gate_part, 'dp', scatter_dimension=0, tiled=True)  28.5 us
    unnamed x2, blocking collectives  14.7 us
    all_gather x2, blocking collectives, single_layer(): lax.all_gather(mixed, 'dp', axis=0, tiled=True)  11.6 us
    reduce_scatter x2, waiting for transfers between devices, single_layer(): lax.psum_scatter(input_part, 'dp', scatter_dimension=0, tiled=True)  10.6 us
    unnamed x40, local copies, waits for them, and re-layouts  8.03 us
    dot_general x2, matrix products, single_layer(): jnp.dot(scaled_in, input_matrix_weight, preferred_element_type=jnp.float32)  5.28 us
  transfers between devices with their start and end apart: 4, of which 3 were waited for; matrix products, arithmetic and copies ran while one was open for 17% of the time, Pallas kernels for 0%

commit v1 on v0

--- a/solution.py
+++ b/solution.py
@@ -120,7 +120,9 @@
     )
     mixed = (y_vals * jax.nn.sigmoid(gate_vals.astype(jnp.float32))).astype(jnp.bfloat16)
     branch_terms = jnp.dot(
-        lax.all_gather(mixed, "dp", axis=0, tiled=True),
+        jnp.concatenate(
+            lax.all_to_all(jnp.stack([mixed] * lax.axis_size("dp")), "dp", 0, 0), axis=0
+        ),
         output_matrix_weight,
         preferred_element_type=jnp.float32,
     )

time: 221 us -> 229 us (1.036)
  matrix products: 24.2 us -> 28.8 us
  starting transfers between devices: 0.16 us -> 4.21 us
  blocking collectives: 114 us -> 111 us
    all_gather x2 -> x0, blocking collectives: 11.6 us -> none  [single_layer(): lax.all_gather(mixed, 'dp', axis=0, tiled=True)]
    all_to_all x0 -> x1, blocking collectives: none -> 8.39 us  [single_layer(): lax.all_to_all(jnp.stack([mixed] * lax.axis_size('dp')), 'dp', 0, 0)]
    all_to_all x0 -> x1, starting transfers between devices: none -> 4.05 us  [single_layer(): lax.all_to_all(jnp.stack([mixed] * lax.axis_size('dp')), 'dp', 0, 0)]
    all_to_all x0 -> x1, waiting for transfers between devices: none -> 2.92 us  [single_layer(): lax.all_to_all(jnp.stack([mixed] * lax.axis_size('dp')), 'dp', 0, 0)]
    unnamed x40 -> x44, local copies, waits for them, and re-layouts: 8.03 us -> 5.74 us
  transfers between devices with their start and end apart: 4 -> 5, of which waited for: 3 -> 4; matrix products, arithmetic and copies ran while one was open for 17% -> 18% of each run, Pallas kernels for 0% -> 0%
where the time goes in v1:
time: 229 us; the launch traced here: 228 us
  blocking collectives  111 us (48%)
  waiting for transfers between devices  41.3 us (18%)
  matrix products  28.8 us (13%)
  local copies, waits for them, and re-layouts  18.5 us (8%)
  between operations  14.8 us (6%)
  other arithmetic  10 us (4%)
  starting transfers between devices  4.21 us (2%)
    psum x2, blocking collectives, single_layer(): branch = lax.psum(branch_terms, 'tp').astype(jnp.bfloat16)  87.8 us
    reduce_scatter x2, waiting for transfers between devices, single_layer(): lax.psum_scatter(gate_part, 'dp', scatter_dimension=0, tiled=True)  28.9 us
    unnamed x2, blocking collectives  14.6 us
    reduce_scatter x2, waiting for transfers between devices, single_layer(): lax.psum_scatter(input_part, 'dp', scatter_dimension=0, tiled=True)  9.49 us
    all_to_all x1, blocking collectives, single_layer(): lax.all_to_all(jnp.stack([mixed] * lax.axis_size('dp')), 'dp', 0, 0)  8.39 us
    dot_general x2, matrix products, state_space_update(): jnp.einsum('tkl,klf->tkf', input_groups, input_real, precision=TOP_PRECIS...  5.9 us
    unnamed x44, local copies, waits for them, and re-layouts  5.74 us
    dot_general x2, matrix products, single_layer(): jnp.dot(scaled_in, input_matrix_weight, preferred_element_type=jnp.float32)  5.3 us
  transfers between devices with their start and end apart: 5, of which 4 were waited for; matrix products, arithmetic and copies ran while one was open for 18% of the time, Pallas kernels for 0%

profile of v1, /device:TPU:0, one launch (start us, length us, event | category | flops | bytes accessed | tf_op | source)
XLA Modules:
  0.0 228.4 jit_solution(17391862203603881752)
XLA Ops:
  7.2 0.8 fusion.85
  8.0 2.6 %fusion.28 = f32[256,512]{1,0:T(8,128)} fusion(bf16[2,1024,512]{2,1,0:T(8,128)(2,1)} %param.20, bf16[256,1024]{1,0:T(8,128)(2,1)} %param.16, f32[1024]{0:T(1024)S(1)} %bitcast.106), kind=kOutput, calls=%fused_computation.51 | convolution fusion | flops 269221888 | bytes 2101248 | tf_op jit(solution)/shard_map/dot_general | solution.py:93
  10.8 2.6 %fusion.26 = f32[256,512]{1,0:T(8,128)} fusion(bf16[2,1024,512]{2,1,0:T(8,128)(2,1)} %param.21, bf16[256,1024]{1,0:T(8,128)(2,1)S(1)} %copy-done.3, f32[1024]{0:T(1024)S(1)} %bitcast.107), kind=kOutput, calls=%fused_computation.49 | convolution fusion | flops 269221888 | bytes 2101248 | tf_op jit(solution)/shard_map/dot_general | solution.py:94
  13.4 0.2 fusion.13
  13.6 8.5 %all-reduce = f32[256]{0:T(256)S(1)} all-reduce(f32[256]{0:T(256)S(1)} %fusion.13), channel_id=3, replica_groups=mesh['grp'=2,'tp'=4,'dp'=4] {'dp'}, use_global_device_ids=true, to_apply=%region_2.4.clone | all-reduce | flops 256 | bytes 2048
  22.2 0.6 fusion.86
  22.8 0.1 slice_reduce_fusion
  22.9 0.1 reshape_squeeze.13
  22.9 0.1 reshape_squeeze.12
  23.0 0.8 slice_bitcast_fusion.1
  23.8 0.7 slice_bitcast_fusion
  24.6 0.1 fusion.84
  24.7 0.6 copy.53
  25.3 1.9 copy.51
  27.2 0.6 gather_fusion.1
  27.8 2.2 gather_fusion
  30.0 0.1 fusion.72
  30.1 0.1 copy.41
  30.1 1.7 fusion.83
  31.9 0.6 dynamic-slice
  33.1 0.1 fusion.80
  33.2 2.5 %copy_bitcast_fusion = (f32[64,32,128]{2,0,1:T(8,128)}, f32[64,32,128]{2,0,1:T(8,128)}) fusion(f32[1,64,32,128]{3,2,1,0:T(8,128)S(1)} %get-tuple-element.21, f32[1,64,32,128]{3,2,1,0:T(8,128)S(1)} %get-tuple-element.22), kind=kLoop, calls=%fused_computation.39 | loop fusion | bytes 4194304 | tf_op jit(solution)/shard_map/squeeze | solution.py:156
  35.8 0.2 exponential_multiply_fusion.1
  36.0 1.0 multiply_convert_fusion.3
  37.0 0.1 copy.43
  37.1 0.8 fusion.50
  37.9 2.9 %fusion.5 = (f32[64,32,64]{2,0,1:T(8,128)S(1)}, f32[64,32,64]{2,0,1:T(8,128)S(1)}) fusion(f32[32,64,64]{2,1,0:T(8,128)S(1)} %fusion.50, f32[64,32,128]{2,0,1:T(8,128)} %get-tuple-element.46, f32[32,64]{1,0:T(8,128)S(1)} %get-tuple-element.36, f32[32,64]{1,0:T(8,128)S(1)} %get-tuple-element.35, f32[32,64]{1,0:T(8,128)S(1)} %get-tuple-element.34, ...), kind=kOutput, calls=%fused_computation.24 | convolution fusion | flops 27262976 | bytes 2990080 | tf_op jit(solution)/shard_map/tkl,klf->tkf/dot_general | solution.py:44
  40.9 1.7 fusion.48
  42.6 1.8 convolution_subtract_fusion.1
  44.4 0.1 copy.44
  44.5 15.1 %reduce-scatter.7.cloned.1.call-done = f32[64,512]{1,0:T(8,128)} async-done(((f32[256,512]{1,0:T(8,128)}), f32[64,512]{1,0:T(8,128)}) %reduce-scatter.7.cloned.1.call-update) | async-done | bytes 131088 | tf_op jit(solution)/shard_map/reduce_scatter | solution.py:98
  59.6 1.1 fusion.62
  60.7 8.4 %all_to_all.10 = bf16[4,64,512]{2,1,0:T(8,128)(2,1)S(1)} all-to-all(bf16[4,64,512]{2,1,0:T(8,128)(2,1)S(1)} %stack.10), channel_id=1, replica_groups=mesh['grp'=2,'tp'=4,'dp'=4] {'dp'}, dimensions={0} | all-to-all | bytes 524288 | tf_op jit(solution)/shard_map/all_to_all | solution.py:124
  69.1 1.7 fusion.24
  70.8 44.2 %all-reduce.4 = bf16[256,1024]{1,0:T(8,128)(2,1)} all-reduce(f32[256,1024]{1,0:T(8,128)S(1)} %fusion.24), channel_id=1, replica_groups=mesh['grp'=2,'tp'=4,'dp'=4] {'tp'}, use_global_device_ids=true, to_apply=%region_4.0 | all-reduce | flops 262144 | bytes 1572864 | tf_op jit(solution)/shard_map/psum | solution.py:129
  114.9 1.5 fusion.16
  116.4 2.7 %fusion.22 = f32[256,512]{1,0:T(8,128)} fusion(bf16[2,1024,512]{2,1,0:T(8,128)(2,1)} %param.20, bf16[256,1024]{1,0:T(8,128)(2,1)S(1)} %get-tuple-element.14, f32[1024]{0:T(1024)S(1)} %bitcast.104), kind=kOutput, calls=%fused_computation.45 | convolution fusion | flops 269221888 | bytes 2101248 | tf_op jit(solution)/shard_map/dot_general | solution.py:93
  119.2 0.1 reshape_squeeze.15
  119.2 0.1 reshape_squeeze.14
  119.3 0.1 copy.46
  119.4 0.8 exponential_multiply_fusion
  120.2 0.3 maximum_bitcast_fusion
  120.6 6.1 %all-reduce.1 = f32[256]{0:T(256)S(1)} all-reduce(f32[256]{0:T(256)S(1)} %get-tuple-element.13), channel_id=6, replica_groups=mesh['grp'=2,'tp'=4,'dp'=4] {'dp'}, use_global_device_ids=true, to_apply=%region_7.9.clone | all-reduce | flops 256 | bytes 2048
  126.6 0.1 fusion.81
  126.7 2.7 %fusion.20 = f32[256,512]{1,0:T(8,128)} fusion(bf16[2,1024,512]{2,1,0:T(8,128)(2,1)} %param.21, bf16[256,1024]{1,0:T(8,128)(2,1)} %copy-done.2, f32[1024]{0:T(1024)S(1)} %bitcast.105), kind=kOutput, calls=%fused_computation.43 | convolution fusion | flops 269221888 | bytes 2101248 | tf_op jit(solution)/shard_map/dot_general | solution.py:94
  129.4 9.5 %reduce-scatter.9.cloned.1.call-done = f32[64,512]{1,0:T(8,128)} async-done(((f32[256,512]{1,0:T(8,128)}), f32[64,512]{1,0:T(8,128)}) %reduce-scatter.9.cloned.1.call-update) | async-done | bytes 131088 | tf_op jit(solution)/shard_map/reduce_scatter | solution.py:97
  138.9 1.0 multiply_convert_fusion.1
  139.9 0.1 copy.48
  140.0 0.8 fusion.43
  140.8 3.0 %fusion.11 = (f32[64,32,64]{2,0,1:T(8,128)S(1)}, f32[64,32,64]{2,0,1:T(8,128)S(1)}) fusion(f32[32,64,64]{2,1,0:T(8,128)S(1)} %fusion.43, f32[64,32,128]{2,0,1:T(8,128)} %get-tuple-element.45, f32[32,64]{1,0:T(8,128)} %get-tuple-element.32, f32[32,64]{1,0:T(8,128)} %get-tuple-element.31, f32[32,64]{1,0:T(8,128)} %get-tuple-element.30, ...), kind=kOutput, calls=%fused_computation.30 | convolution fusion | flops 27262976 | bytes 2990080 | tf_op jit(solution)/shard_map/tkl,klf->tkf/dot_general | solution.py:44
  143.8 1.7 fusion.41
  145.5 2.5 %convolution_subtract_fusion = f32[32,64,16]{1,2,0:T(8,128)} fusion(f32[32,64,16]{1,2,0:T(8,128)S(1)} %fusion.41, f32[64,32,64]{2,0,1:T(8,128)S(1)} %get-tuple-element.17, f32[32,16,128]{2,1,0:T(8,128)S(1)} %get-tuple-element.25), kind=kOutput, calls=%fused_computation.17 | convolution fusion | flops 25198592 | bytes 1048576 | tf_op jit(solution)/shard_map/hzk,dhk->dhz/dot_general | solution.py:68
  148.1 1.1 copy.49
  149.1 13.8 %reduce-scatter.11.cloned.1.call-done = f32[64,512]{1,0:T(8,128)} async-done(((f32[256,512]{1,0:T(8,128)}), f32[64,512]{1,0:T(8,128)}) %reduce-scatter.11.cloned.1.call-update) | async-done | bytes 131088 | tf_op jit(solution)/shard_map/reduce_scatter | solution.py:98
  162.9 1.1 fusion.71
  164.0 0.7 stack.11
  164.7 4.1 %all-to-all-start.1 = ((bf16[4,64,512]{2,1,0:T(8,128)(2,1)}), bf16[4,64,512]{2,1,0:T(8,128)(2,1)}, u32[]{:S(2)}, u32[]{:S(2)}) async-start(bf16[4,64,512]{2,1,0:T(8,128)(2,1)} %stack.11), calls=%async_computation.5 | async-start | bytes 524288 | tf_op jit(solution)/shard_map/all_to_all | solution.py:124
  168.8 0.3 maximum_bitcast_fusion.1
  169.1 0.2 pad_maximum_fusion
  169.4 2.5 %copy.50 = f32[2,64,32,128]{3,2,1,0:T(8,128)} copy(f32[2,64,32,128]{3,1,2,0:T(8,128)S(1)} %pad_maximum_fusion) | data formatting | bytes 4194304
  171.9 2.9 %all-to-all-done.1 = bf16[4,64,512]{2,1,0:T(8,128)(2,1)} async-done(((bf16[4,64,512]{2,1,0:T(8,128)(2,1)}), bf16[4,64,512]{2,1,0:T(8,128)(2,1)}, u32[]{:S(2)}, u32[]{:S(2)}) %all-to-all-start.1) | async-done | bytes 262176 | tf_op jit(solution)/shard_map/all_to_all | solution.py:124
  174.8 1.4 fusion.18
  176.2 43.6 %all-reduce.5 = bf16[256,1024]{1,0:T(8,128)(2,1)S(1)} all-reduce(f32[256,1024]{1,0:T(8,128)S(1)} %fusion.18), channel_id=1, replica_groups=mesh['grp'=2,'tp'=4,'dp'=4] {'tp'}, use_global_device_ids=true, to_apply=%region_9.11 | all-reduce | flops 262144 | bytes 1572864 | tf_op jit(solution)/shard_map/psum | solution.py:129
  219.8 2.0 fusion.17
  (53 shorter events, 0.4 us)
Async XLA Ops:
  7.2 3.6 %copy-start.3 = (bf16[256,1024]{1,0:T(8,128)(2,1)S(1)}, bf16[256,1024]{1,0:T(8,128)(2,1)}, u32[]{:S(2)}) copy-start(bf16[256,1024]{1,0:T(8,128)(2,1)} %param.16) | copy-start | bytes 1572868
  7.2 28.8 %reduce-scatter.5.cloned.1.call-start = ((), (), s32[]{:S(2)}) async-start(), calls=%async_computation.6 | async-start | bytes 655360 | tf_op jit(solution)/shard_map/reduce_scatter | solution.py:97
  10.6 11.5 %copy-start.18 = (s32[64]{0:T(128)S(1)}, s32[64]{0:T(128)}, u32[]{:S(2)}) copy-start(s32[64]{0:T(128)} %param.17) | copy-start | bytes 772
  10.6 11.5 %copy-start.17 = (f32[2,32]{1,0:T(2,128)S(1)}, f32[2,32]{1,0:T(2,128)}, u32[]{:S(2)}) copy-start(f32[2,32]{1,0:T(2,128)} %param.25) | copy-start | bytes 772
  10.6 11.5 %copy-start.14 = (f32[2,512]{1,0:T(2,128)S(1)}, f32[2,512]{1,0:T(2,128)}, u32[]{:S(2)}) copy-start(f32[2,512]{1,0:T(2,128)} %param.28) | copy-start | bytes 12292
  10.6 12.1 %copy-start.11 = (f32[2,2048]{1,0:T(2,128)S(1)}, f32[2,2048]{1,0:T(2,128)}, u32[]{:S(2)}) copy-start(f32[2,2048]{1,0:T(2,128)} %param.24) | copy-start | bytes 49156
  10.7 12.1 %copy-start.12 = (f32[2,2048]{1,0:T(2,128)S(1)}, f32[2,2048]{1,0:T(2,128)}, u32[]{:S(2)}) copy-start(f32[2,2048]{1,0:T(2,128)} %param.23) | copy-start | bytes 49156
  10.7 12.3 %copy-start.7 = (f32[2,32,16,128]{3,2,1,0:T(8,128)S(1)}, f32[2,32,16,128]{3,2,1,0:T(8,128)}, u32[]{:S(2)}) copy-start(f32[2,32,16,128]{3,2,1,0:T(8,128)} %param.26) | copy-start | bytes 1572868
  10.7 13.1 %copy-start.8 = (f32[2,32,16,128]{3,2,1,0:T(8,128)S(1)}, f32[2,32,16,128]{3,2,1,0:T(8,128)}, u32[]{:S(2)}) copy-start(f32[2,32,16,128]{3,2,1,0:T(8,128)} %param.27) | copy-start | bytes 1572868
  10.7 48.9 %reduce-scatter.7.cloned.1.call-start = ((), (), s32[]{:S(2)}) async-start(), calls=%async_computation.7 | async-start | bytes 655360 | tf_op jit(solution)/shard_map/reduce_scatter | solution.py:98
  13.3 11.2 %copy-start.4 = (f32[2,32,4096]{2,1,0:T(8,128)S(1)}, f32[2,32,4096]{2,1,0:T(8,128)}, u32[]{:S(2)}) copy-start(f32[2,32,4096]{2,1,0:T(8,128)} %param.29) | copy-start | bytes 3145732
  13.4 125.5 %reduce-scatter.9.cloned.1.call-start = ((), (), s32[]{:S(2)}) async-start(), calls=%async_computation.8 | async-start | bytes 655360 | tf_op jit(solution)/shard_map/reduce_scatter | solution.py:97
  30.1 1.8 copy-start.19
  33.2 3.9 %copy-start.6 = (f32[32,16,128]{2,1,0:T(8,128)S(1)}, f32[32,16,128]{2,1,0:T(8,128)}, u32[]{:S(2)}) copy-start(f32[32,16,128]{2,1,0:T(8,128)} %get-tuple-element.28) | copy-start | bytes 786436
  37.9 3.0 %copy-start = (f32[32,16,128]{2,1,0:T(8,128)S(1)}, f32[32,16,128]{2,1,0:T(8,128)}, u32[]{:S(2)}) copy-start(f32[32,16,128]{2,1,0:T(8,128)} %get-tuple-element.26) | copy-start | bytes 786436
  40.8 18.8 %copy-start.9 = (f32[64,512]{1,0:T(8,128)S(1)}, f32[64,512]{1,0:T(8,128)}, u32[]{:S(2)}) copy-start(f32[64,512]{1,0:T(8,128)} %reduce-scatter.5.cloned.1.call-done) | copy-start | bytes 393220
  116.4 3.0 %copy-start.2 = (bf16[256,1024]{1,0:T(8,128)(2,1)}, bf16[256,1024]{1,0:T(8,128)(2,1)S(1)}, u32[]{:S(2)}) copy-start(bf16[256,1024]{1,0:T(8,128)(2,1)S(1)} %get-tuple-element.14) | copy-start | bytes 1572868
  119.1 43.8 %reduce-scatter.11.cloned.1.call-start = ((), (), s32[]{:S(2)}) async-start(), calls=%async_computation.9 | async-start | bytes 655360 | tf_op jit(solution)/shard_map/reduce_scatter | solution.py:98
  120.6 19.4 %copy-start.5 = (f32[32,16,128]{2,1,0:T(8,128)S(1)}, f32[32,16,128]{2,1,0:T(8,128)}, u32[]{:S(2)}) copy-start(f32[32,16,128]{2,1,0:T(8,128)} %get-tuple-element.27) | copy-start | bytes 786436
  126.7 12.2 %copy-start.15 = (f32[64]{0:T(128)}, f32[64]{0:T(128)S(1)}, u32[]{:S(2)}) copy-start(f32[64]{0:T(128)S(1)} %fusion.81) | copy-start | bytes 772
  143.8 19.1 %copy-start.10 = (f32[64,512]{1,0:T(8,128)S(1)}, f32[64,512]{1,0:T(8,128)}, u32[]{:S(2)}) copy-start(f32[64,512]{1,0:T(8,128)} %reduce-scatter.9.cloned.1.call-done) | copy-start | bytes 393220
  143.8 19.1 %copy-start.13 = (f32[1,512]{1,0:T(1,128)S(1)}, f32[1,512]{1,0:T(1,128)}, u32[]{:S(2)}) copy-start(f32[1,512]{1,0:T(1,128)} %get-tuple-element.39) | copy-start | bytes 6148
  143.8 19.1 %copy-start.16 = (f32[64]{0:T(128)S(1)}, f32[64]{0:T(128)}, u32[]{:S(2)}) copy-start(f32[64]{0:T(128)} %copy-done.15) | copy-start | bytes 772
  164.7 10.1 %all-to-all-start.1 = ((bf16[4,64,512]{2,1,0:T(8,128)(2,1)}), bf16[4,64,512]{2,1,0:T(8,128)(2,1)}, u32[]{:S(2)}, u32[]{:S(2)}) async-start(bf16[4,64,512]{2,1,0:T(8,128)(2,1)} %stack.11), calls=%async_computation.5 | async-start | bytes 524288 | tf_op jit(solution)/shard_map/all_to_all | solution.py:124
  169.4 5.5 %copy-start.1 = (bf16[2,512,1024]{2,1,0:T(8,128)(2,1)S(1)}, bf16[2,512,1024]{2,1,0:T(8,128)(2,1)}, u32[]{:S(2)}) copy-start(bf16[2,512,1024]{2,1,0:T(8,128)(2,1)} %param.22) | copy-start | bytes 6291460
Sparse Core Ops, SparseCore 0:
  11.0 24.3 reduce-scatter.4
  37.9 21.6 reduce-scatter.6
  119.2 19.5 reduce-scatter.8
  141.2 21.6 reduce-scatter.10
